TPU v7x, 32 devices: a whole 2x2x4 slice. The times are simulated.
32 devices in a mesh: sp: 8 (over z, y), dp: 4 (over x, core).
Axes of the slice: x: 2, y: 2, z: 4, core: 2. Of those that a mesh axis runs over, the one named last changes fastest.
Arguments:
- tokens: bfloat16 [4, 2560, 2048], P('dp', 'sp'), may hold values from -6 to 6
- w_query: bfloat16 [2048, 1024], P('dp', 'sp'), may hold values from -0.125 to 0.125
- w_key: bfloat16 [2048, 1024], P('dp', 'sp'), may hold values from -0.125 to 0.125
- w_value: bfloat16 [2048, 1024], P('dp', 'sp'), may hold values from -0.125 to 0.125
- w_output: bfloat16 [1024, 2048], P('sp', 'dp'), may hold values from -0.1875 to 0.1875
- qk_gain: float32 [2, 64], replicated, may hold values from 0.4 to 7
- decay_sums: float32 [4, 16, 2560], P('dp', 'sp'), may hold values from -512 to 0, as said below
Outputs:
- layer_out: bfloat16 [4, 2560, 2048], P('dp', 'sp')
Inputs may be any that keep to these rules, and one draw needn't show every extreme that they name: `decay_sums`: each row is non-increasing along positions.
All inputs are finite; a program needn't handle non-finite values.
Results may differ from a plain program's by a relative error of at most 0.0075.
The roundings to bfloat16 on the way count: a program that leaves them out, or rounds other values in their place, can miss the bound.
Values may be sent and summed in bfloat16 or wider, within the bound.
A program may use at most 128 MiB of HBM per device.

v0:
```python
import jax
import jax.numpy as jnp
from jax import lax
from jax.sharding import PartitionSpec as P


def normalize(values):
    values = values.astype(jnp.float32)
    return values * lax.rsqrt(jnp.mean(values * values, axis=-1, keepdims=True) + 1e-06)


def attend(query_unit, key_unit, value_rows, decay_rows):
    length = query_unit.shape[0]
    groups = query_unit.shape[1]
    width = query_unit.shape[2]
    block = min(512, length)

    def one_block(index):
        start = index * block
        query_block = lax.dynamic_slice_in_dim(query_unit, start, block, 0)
        decay_block = lax.dynamic_slice_in_dim(decay_rows, start, block, 1)
        query_place = start + jnp.arange(block, dtype=jnp.int32)

        def fill(column, buffer):
            key_start = column * block
            key_block = lax.dynamic_slice_in_dim(key_unit, key_start, block, 0)
            decay_keys = lax.dynamic_slice_in_dim(decay_rows, key_start, block, 1)
            scores = jnp.einsum(
                "qhd,khd->hqk", query_block, key_block, preferred_element_type=jnp.float32
            )
            scores = scores + decay_block[:, :, None] - decay_keys[:, None, :]
            key_place = key_start + jnp.arange(block, dtype=jnp.int32)
            scores = jnp.where(
                key_place[None, None, :] <= query_place[None, :, None], scores, -jnp.inf
            )
            return lax.dynamic_update_slice_in_dim(buffer, scores, key_start, 2)

        empty = jnp.full((groups, block, length), -jnp.inf, jnp.float32)
        scores = lax.fori_loop(0, index + 1, fill, empty)
        peak = jnp.max(scores, axis=-1, keepdims=True)
        weights = jnp.exp(scores - peak)
        probs = (weights / jnp.sum(weights, axis=-1, keepdims=True)).astype(jnp.bfloat16)

        def gather_values(column, running):
            key_start = column * block
            prob_block = lax.dynamic_slice_in_dim(probs, key_start, block, 2)
            value_block = lax.dynamic_slice_in_dim(value_rows, key_start, block, 0)
            return running + jnp.einsum(
                "hqk,khd->qhd", prob_block, value_block, preferred_element_type=jnp.float32
            )

        zeros = jnp.zeros((block, groups, width), jnp.float32)
        return lax.fori_loop(0, index + 1, gather_values, zeros)

    blocks = lax.map(one_block, jnp.arange(length // block, dtype=jnp.int32))
    return blocks.reshape(length, groups, width)


def on_device(tokens, w_query, w_key, w_value, w_output, qk_gain, decay_sums):
    own_rows = tokens[0]
    decay_rows = decay_sums[0]
    head_group = decay_rows.shape[0]
    head_dim = qk_gain.shape[1]
    stacked = jnp.stack((w_query, w_key, w_value))
    columns, out_columns = (
        lax.all_gather(stacked, "dp", axis=1, tiled=True),
        lax.all_gather(w_output, "dp", axis=1, tiled=True),
    )
    whole = lax.all_gather(own_rows, "sp", axis=0, tiled=True)
    triple = jnp.einsum("td,kdc->ktc", whole, columns, preferred_element_type=jnp.float32).astype(
        jnp.bfloat16
    )
    length = triple.shape[1]
    grouped = triple.reshape(3, length, head_group, head_dim)
    query_unit = (normalize(grouped[0]) * qk_gain[0] * head_dim ** (-0.5)).astype(jnp.bfloat16)
    key_unit = (normalize(grouped[1]) * qk_gain[1]).astype(jnp.bfloat16)
    attended = attend(query_unit, key_unit, grouped[2], decay_rows)
    head_out = normalize(attended).astype(jnp.bfloat16).reshape(length, head_group * head_dim)
    merged = lax.all_to_all(head_out, "sp", split_axis=0, concat_axis=1, tiled=True)
    result = jnp.dot(
        merged,
        lax.all_gather(out_columns, "sp", axis=0, tiled=True),
        preferred_element_type=jnp.float32,
    )
    return result.astype(jnp.bfloat16)[None]


def solution(mesh):
    placed = (
        P("dp", "sp", None),
        P("dp", "sp"),
        P("dp", "sp"),
        P("dp", "sp"),
        P("sp", "dp"),
        P(),
        P("dp", "sp", None),
    )
    return jax.shard_map(
        on_device, mesh=mesh, in_specs=placed, out_specs=P("dp", "sp", None), check_vma=False
    )
```

profile of v0, /device:TPU:0, one launch (start us, length us, event | category | flops | bytes accessed | tf_op | source)
XLA Modules:
  0.0 412.7 jit_solution(10661305282785432766)
XLA Ops:
  11.3 9.1 %all_gather.14 = bf16[128,2048]{1,0:T(8,128)(2,1)} all-gather(bf16[128,512]{1,0:T(8,128)(2,1)S(1)} %copy-done.1), channel_id=1, replica_groups=mesh['sp'=8,'dp'=4] {'dp'}, dimensions={1}, use_global_device_ids=true | all-gather | bytes 655360 | tf_op jit(solution)/shard_map/all_gather | solution.py:67
  20.4 12.5 %all-gather.5.cloned.1.call-done = bf16[3,2048,128]{1,2,0:T(8,128)(2,1)} async-done(((bf16[3,512,128]{1,2,0:T(8,128)(2,1)}), bf16[3,2048,128]{1,2,0:T(8,128)(2,1)}) %all-gather.5.cloned.1.call-update) | async-done | bytes 1572880 | tf_op jit(solution)/shard_map/all_gather | solution.py:66
  33.0 152.7 %all-gather.9.cloned.1.call-done = bf16[1,2560,2048]{2,1,0:T(8,128)(2,1)} async-done(((bf16[1,320,2048]{2,1,0:T(8,128)(2,1)}), bf16[1,2560,2048]{2,1,0:T(8,128)(2,1)}) %all-gather.9.cloned.1.call-update) | async-done | bytes 10485776 | tf_op jit(solution)/shard_map/all_gather | solution.py:69
  185.7 8.7 %fusion.17 = bf16[3,2560,128]{1,2,0:T(8,128)(2,1)S(1)} fusion(bf16[3,2048,128]{1,2,0:T(8,128)(2,1)} %all-gather.5.cloned.1.call-done, bf16[1,2560,2048]{2,1,0:T(8,128)(2,1)} %all-gather.9.cloned.1.call-done), kind=kOutput, calls=%fused_computation.25 | convolution fusion | flops 4027514880 | bytes 14024704 | tf_op jit(solution)/shard_map/td,kdc->ktc/dot_general | solution.py:70
  195.3 176.2 %while.33 = (s32[]{:T(128)}, f32[5,512,2,64]{1,3,2,0:T(8,128)S(1)}, s32[5]{0:T(128)S(1)}, bf16[2560,2,64]{0,2,1:T(8,128)(2,1)S(1)}, f32[2,2560]{1,0:T(2,128)}, /...) while((s32[]{:T(128)}, f32[5,512,2,64]{1,3,2,0:T(8,128)S(1)}, ...), condition=%wide.region_9.10_spmd, body=%wide.region_2.9_spmd.sunk | while | flops 143990816 | bytes 31886096 | solution.py:55
  198.1 5.3 %broadcast.99 = f32[2,512,2560]{1,2,0:T(8,128)} broadcast(f32[]{:T(128)} %constant.14.clone.6..sunk), dimensions={} | broadcast | bytes 10485764 | tf_op jit(solution)/shard_map/broadcast.5
  206.3 13.8 %divide_convert_fusion.2 = bf16[2,512,2560]{1,2,0:T(8,128)(2,1)} fusion(f32[2,512,2560]{1,2,0:T(8,128)} %get-tuple-element.345), kind=kOutput, calls=%fused_computation.16.clone.1 | output fusion | flops 7871486 | bytes 15728640 | tf_op jit(solution)/shard_map/while/body/eval_jaxpr/div | solution.py:42
  224.4 5.3 %broadcast.99 = f32[2,512,2560]{1,2,0:T(8,128)} broadcast(f32[]{:T(128)} %constant.14.clone.6..sunk), dimensions={} | broadcast | bytes 10485764 | tf_op jit(solution)/shard_map/broadcast.5
  229.7 5.8 %while.34 = (s32[]{:T(128)}, f32[2,512,2560]{1,2,0:T(8,128)}, s32[]{:T(128)}, bf16[2560,2,64]{0,2,1:T(8,128)(2,1)S(1)}, bf16[512,2,64]{0,2,1:T(8,128)(2,1)S(1)},...) while((s32[]{:T(128)}, f32[2,512,2560]{1,2,0:T(8,128)}, ...), condition=%wide.region_4.4_spmd.clone, body=%wide.region_3.3_spmd.clone.sunk | while | flops 68944904 | bytes 2909359 | solution.py:39
  235.5 13.8 %divide_convert_fusion.2 = bf16[2,512,2560]{1,2,0:T(8,128)(2,1)} fusion(f32[2,512,2560]{1,2,0:T(8,128)} %get-tuple-element.345), kind=kOutput, calls=%fused_computation.16.clone.1 | output fusion | flops 7871486 | bytes 15728640 | tf_op jit(solution)/shard_map/while/body/eval_jaxpr/div | solution.py:42
  255.1 5.3 %broadcast.99 = f32[2,512,2560]{1,2,0:T(8,128)} broadcast(f32[]{:T(128)} %constant.14.clone.6..sunk), dimensions={} | broadcast | bytes 10485764 | tf_op jit(solution)/shard_map/broadcast.5
  260.4 8.7 %while.34 = (s32[]{:T(128)}, f32[2,512,2560]{1,2,0:T(8,128)}, s32[]{:T(128)}, bf16[2560,2,64]{0,2,1:T(8,128)(2,1)S(1)}, bf16[512,2,64]{0,2,1:T(8,128)(2,1)S(1)},...) while((s32[]{:T(128)}, f32[2,512,2560]{1,2,0:T(8,128)}, ...), condition=%wide.region_4.4_spmd.clone, body=%wide.region_3.3_spmd.clone.sunk | while | flops 68944904 | bytes 2909359 | solution.py:39
  269.1 13.8 %divide_convert_fusion.2 = bf16[2,512,2560]{1,2,0:T(8,128)(2,1)} fusion(f32[2,512,2560]{1,2,0:T(8,128)} %get-tuple-element.345), kind=kOutput, calls=%fused_computation.16.clone.1 | output fusion | flops 7871486 | bytes 15728640 | tf_op jit(solution)/shard_map/while/body/eval_jaxpr/div | solution.py:42
  282.9 4.7 %while.35 = (s32[]{:T(128)}, f32[512,2,64]{0,2,1:T(8,128)S(1)}, s32[]{:T(128)}, bf16[2560,2,64]{0,2,1:T(8,128)(2,1)S(1)}, bf16[2,512,2560]{1,2,0:T(8,128)(2,1)},...) while((s32[]{:T(128)}, f32[512,2,64]{0,2,1:T(8,128)S(1)}, s32[]{:T(128)}, ...), condition=%wide.region_8.8_spmd, body=%wide.region_7.7_spmd.sunk | while | flops 67174408 | bytes 1705099 | solution.py:53
  290.3 5.3 %broadcast.99 = f32[2,512,2560]{1,2,0:T(8,128)} broadcast(f32[]{:T(128)} %constant.14.clone.6..sunk), dimensions={} | broadcast | bytes 10485764 | tf_op jit(solution)/shard_map/broadcast.5
  295.6 11.7 %while.34 = (s32[]{:T(128)}, f32[2,512,2560]{1,2,0:T(8,128)}, s32[]{:T(128)}, bf16[2560,2,64]{0,2,1:T(8,128)(2,1)S(1)}, bf16[512,2,64]{0,2,1:T(8,128)(2,1)S(1)},...) while((s32[]{:T(128)}, f32[2,512,2560]{1,2,0:T(8,128)}, ...), condition=%wide.region_4.4_spmd.clone, body=%wide.region_3.3_spmd.clone.sunk | while | flops 68944904 | bytes 2909359 | solution.py:39
  307.2 13.8 %divide_convert_fusion.2 = bf16[2,512,2560]{1,2,0:T(8,128)(2,1)} fusion(f32[2,512,2560]{1,2,0:T(8,128)} %get-tuple-element.345), kind=kOutput, calls=%fused_computation.16.clone.1 | output fusion | flops 7871486 | bytes 15728640 | tf_op jit(solution)/shard_map/while/body/eval_jaxpr/div | solution.py:42
  321.1 6.3 %while.35 = (s32[]{:T(128)}, f32[512,2,64]{0,2,1:T(8,128)S(1)}, s32[]{:T(128)}, bf16[2560,2,64]{0,2,1:T(8,128)(2,1)S(1)}, bf16[2,512,2560]{1,2,0:T(8,128)(2,1)},...) while((s32[]{:T(128)}, f32[512,2,64]{0,2,1:T(8,128)S(1)}, s32[]{:T(128)}, ...), condition=%wide.region_8.8_spmd, body=%wide.region_7.7_spmd.sunk | while | flops 67174408 | bytes 1705099 | solution.py:53
  330.0 5.3 %broadcast.99 = f32[2,512,2560]{1,2,0:T(8,128)} broadcast(f32[]{:T(128)} %constant.14.clone.6..sunk), dimensions={} | broadcast | bytes 10485764 | tf_op jit(solution)/shard_map/broadcast.5
  335.3 14.5 %while.34 = (s32[]{:T(128)}, f32[2,512,2560]{1,2,0:T(8,128)}, s32[]{:T(128)}, bf16[2560,2,64]{0,2,1:T(8,128)(2,1)S(1)}, bf16[512,2,64]{0,2,1:T(8,128)(2,1)S(1)},...) while((s32[]{:T(128)}, f32[2,512,2560]{1,2,0:T(8,128)}, ...), condition=%wide.region_4.4_spmd.clone, body=%wide.region_3.3_spmd.clone.sunk | while | flops 68944904 | bytes 2909359 | solution.py:39
  349.8 13.8 %divide_convert_fusion.2 = bf16[2,512,2560]{1,2,0:T(8,128)(2,1)} fusion(f32[2,512,2560]{1,2,0:T(8,128)} %get-tuple-element.345), kind=kOutput, calls=%fused_computation.16.clone.1 | output fusion | flops 7871486 | bytes 15728640 | tf_op jit(solution)/shard_map/while/body/eval_jaxpr/div | solution.py:42
  363.7 7.8 %while.35 = (s32[]{:T(128)}, f32[512,2,64]{0,2,1:T(8,128)S(1)}, s32[]{:T(128)}, bf16[2560,2,64]{0,2,1:T(8,128)(2,1)S(1)}, bf16[2,512,2560]{1,2,0:T(8,128)(2,1)},...) while((s32[]{:T(128)}, f32[512,2,64]{0,2,1:T(8,128)S(1)}, s32[]{:T(128)}, ...), condition=%wide.region_8.8_spmd, body=%wide.region_7.7_spmd.sunk | while | flops 67174408 | bytes 1705099 | solution.py:53
  384.4 17.0 %all-to-all-done = bf16[8,320,128]{2,1,0:T(8,128)(2,1)S(1)} async-done(((bf16[8,320,128]{2,1,0:T(8,128)(2,1)}), bf16[8,320,128]{2,1,0:T(8,128)(2,1)S(1)}, u32[]{:S(2)}, u32[]{:S(2)}) %all-to-all-start) | async-done | bytes 655392 | tf_op jit(solution)/shard_map/all_to_all | solution.py:79
  401.4 4.8 %fusion.20 = bf16[1,320,2048]{2,1,0:T(8,128)(2,1)} fusion(bf16[1024,2048]{1,0:T(8,128)(2,1)} %all-gather.7.cloned.1.call-done, bf16[8,320,128]{2,1,0:T(8,128)(2,1)S(1)} %all-to-all-done), kind=kOutput, calls=%fused_computation.27 | convolution fusion | flops 1342832640 | bytes 6160384 | tf_op jit(solution)/shard_map/dot_general | solution.py:80
  (138 shorter events, 99.3 us)
Async XLA Ops:
  6.5 4.7 %copy-start.1 = (bf16[128,512]{1,0:T(8,128)(2,1)S(1)}, bf16[128,512]{1,0:T(8,128)(2,1)}, u32[]{:S(2)}) copy-start(bf16[128,512]{1,0:T(8,128)(2,1)} %param.17) | copy-start | bytes 393220
  6.5 26.4 %all-gather.5.cloned.1.call-start = ((), (), s32[]{:S(2)}) async-start(), calls=%async_computation.1 | async-start | bytes 1966080 | tf_op jit(solution)/shard_map/all_gather | solution.py:66
  8.6 11.8 %copy-start.2 = (f32[2,64]{1,0:T(2,128)S(1)}, f32[2,64]{1,0:T(2,128)}, u32[]{:S(2)}) copy-start(f32[2,64]{1,0:T(2,128)} %param.18) | copy-start | bytes 1540
  10.4 175.2 %all-gather.9.cloned.1.call-start = ((), (), s32[]{:S(2)}) async-start(), calls=%async_computation.3 | async-start | bytes 11796480 | tf_op jit(solution)/shard_map/all_gather | solution.py:69
  11.2 373.2 %all-gather.7.cloned.1.call-start = ((), (), s32[]{:S(2)}) async-start(), calls=%async_computation.2 | async-start | bytes 4718592 | tf_op jit(solution)/shard_map/all_gather | solution.py:82
  374.5 2.9 copy-start
  380.8 20.6 %all-to-all-start = ((bf16[8,320,128]{2,1,0:T(8,128)(2,1)}), bf16[8,320,128]{2,1,0:T(8,128)(2,1)S(1)}, u32[]{:S(2)}, u32[]{:S(2)}) async-start(bf16[8,320,128]{2,1,0:T(8,128)(2,1)} %copy.29), calls=%async_computation | async-start | bytes 1310720 | tf_op jit(solution)/shard_map/all_to_all | solution.py:79
Sparse Core Ops, SparseCore 0:
  10.6 22.3 all-gather.4
  35.1 150.5 all-gather.8
  187.8 70.9 all-gather.6
where the time goes:
time: 414 us; the launch traced here: 413 us
  waiting for transfers between devices  183 us (44%)
  other arithmetic  75.1 us (18%)
  matrix products  66.4 us (16%)
  local copies, waits for them, and re-layouts  54.8 us (13%)
  between operations  13.3 us (3%)
  blocking collectives  9.1 us (2%)
  loops' own time  7.36 us (2%)
    all_gather x1, waiting for transfers between devices, on_device(): whole = lax.all_gather(own_rows, 'sp', axis=0, tiled=True)  153 us
    div x5, other arithmetic, one_block(): weights / jnp.sum(weights, axis=-1, keepdims=True)  69 us
    dot_general x15, matrix products, fill(): jnp.einsum('qhd,khd->hqk', query_block, key_block, preferred_element_type...  29.8 us
    another operation x10, local copies, waits for them, and re-layouts  26.7 us
    dot_general x15, matrix products, gather_values(): jnp.einsum('hqk,khd->qhd', prob_block, value_block, preferred_element_typ...  23.1 us
    all_to_all x1, waiting for transfers between devices, on_device(): lax.all_to_all(head_out, 'sp', split_axis=0, concat_axis=1, tiled=True)  17 us
    all_gather x1, waiting for transfers between devices, on_device(): lax.all_gather(stacked, 'dp', axis=1, tiled=True)  12.5 us
    dynamic_slice x15, local copies, waits for them, and re-layouts, fill(): decay_keys = lax.dynamic_slice_in_dim(decay_rows, key_start, block, 1)  10.3 us
  transfers between devices with their start and end apart: 4, of which 3 were waited for; matrix products, arithmetic and copies ran while one was open for 45% of the time, Pallas kernels for 0%

commit v1 on v0

--- a/solution.py
+++ b/solution.py
@@ -57,6 +57,26 @@
 
 
 def on_device(tokens, w_query, w_key, w_value, w_output, qk_gain, decay_sums):
+
+    def supply_all_the_heaps(buf, net_axis, vec):
+        z1 = lax.axis_size(net_axis)
+        res = lax.axis_index(net_axis)
+        later, current_value, kept_arr = (z1, res, buf.shape[0])
+        front, v1 = ([], [])
+        clean = work_now = buf
+        d = 0
+        while d < later // 2 + 1:
+            front.append(vec(clean, (current_value - d) % later * kept_arr))
+            if 0 < d < later - later // 2:
+                v1.append(vec(work_now, (current_value + d) % later * kept_arr))
+            clean = lax.ppermute(clean, net_axis, [(w, (w + 1) % later) for w in range(later)])
+            work_now = lax.ppermute(
+                work_now, net_axis, [(w, (w - 1) % later) for w in range(later)]
+            )
+            d = d + 1
+        seen_now = jnp.concatenate([*front[::-1], *v1], axis=1)
+        return jnp.roll(seen_now, (current_value - later // 2) * front[0].shape[1], axis=1)
+
     own_rows = tokens[0]
     decay_rows = decay_sums[0]
     head_group = decay_rows.shape[0]
@@ -66,10 +86,13 @@
         lax.all_gather(stacked, "dp", axis=1, tiled=True),
         lax.all_gather(w_output, "dp", axis=1, tiled=True),
     )
-    whole = lax.all_gather(own_rows, "sp", axis=0, tiled=True)
-    triple = jnp.einsum("td,kdc->ktc", whole, columns, preferred_element_type=jnp.float32).astype(
-        jnp.bfloat16
-    )
+    triple = supply_all_the_heaps(
+        own_rows,
+        "sp",
+        lambda part, offset: jnp.einsum(
+            "td,kdc->ktc", part, columns, preferred_element_type=jnp.float32
+        ),
+    ).astype(jnp.bfloat16)
     length = triple.shape[1]
     grouped = triple.reshape(3, length, head_group, head_dim)
     query_unit = (normalize(grouped[0]) * qk_gain[0] * head_dim ** (-0.5)).astype(jnp.bfloat16)

time: 414 us -> 493 us (1.19)
  starting transfers between devices: 3.62 us -> 67.6 us
  waiting for transfers between devices: 183 us -> 145 us
  matrix products: 66.4 us -> 86.2 us
  blocking collectives: 9.1 us -> 27.5 us
  local copies, waits for them, and re-layouts: 54.8 us -> 65.2 us
    all_gather x1 -> x0, waiting for transfers between devices: 153 us -> none  [on_device(): whole = lax.all_gather(own_rows, 'sp', axis=0, tiled=True)]
    ppermute x0 -> x7, waiting for transfers between devices: none -> 145 us  [the longest x4 134 us: supply_all_the_heaps(): lax.ppermute(clean, net_axis, [(w, (w + 1) % later) for w in range(later)])]
    ppermute x0 -> x7, starting transfers between devices: none -> 67.6 us  [the longest x3 59.5 us: supply_all_the_heaps(): lax.ppermute(work_now, net_axis, [(w, (w - 1) % later) for w in range(lat...]
    all_to_all x0 -> x1, blocking collectives: none -> 19.6 us  [on_device(): lax.all_to_all(head_out, 'sp', split_axis=0, concat_axis=1, tiled=True)]
    all_to_all x1 -> x0, waiting for transfers between devices: 17 us -> none  [on_device(): lax.all_to_all(head_out, 'sp', split_axis=0, concat_axis=1, tiled=True)]
    dot_general x15, matrix products: 29.8 us -> 43.6 us  [fill(): jnp.einsum('qhd,khd->hqk', query_block, key_block, preferred_element_type...]
    all_gather x1, waiting for transfers between devices: 12.5 us -> 0.01 us  [on_device(): lax.all_gather(stacked, 'dp', axis=1, tiled=True)]
    dot_general x1 -> x8, matrix products: 8.71 us -> 14.7 us  [on_device(): jnp.einsum('td,kdc->ktc', part, columns, preferred_element_type=jnp.float32)]
  transfers between devices with their start and end apart: 4 -> 9, of which waited for: 3 -> 5; matrix products, arithmetic and copies ran while one was open for 45% -> 46% of each run, Pallas kernels for 0% -> 0%
where the time goes in v1:
time: 493 us; the launch traced here: 491 us
  waiting for transfers between devices  145 us (29%)
  matrix products  86.2 us (17%)
  other arithmetic  79.4 us (16%)
  starting transfers between devices  67.6 us (14%)
  local copies, waits for them, and re-layouts  65.2 us (13%)
  blocking collectives  27.5 us (6%)
  between operations  13.7 us (3%)
  loops' own time  6.89 us (1%)
    ppermute x4, waiting for transfers between devices, supply_all_the_heaps(): lax.ppermute(clean, net_axis, [(w, (w + 1) % later) for w in range(later)])  134 us
    div x5, other arithmetic, one_block(): weights / jnp.sum(weights, axis=-1, keepdims=True)  69.8 us
    ppermute x3, starting transfers between devices, supply_all_the_heaps(): lax.ppermute(work_now, net_axis, [(w, (w - 1) % later) for w in range(lat...  59.5 us
    dot_general x15, matrix products, fill(): jnp.einsum('qhd,khd->hqk', query_block, key_block, preferred_element_type...  43.6 us
    another operation x10, local copies, waits for them, and re-layouts  26.8 us
    dot_general x15, matrix products, gather_values(): jnp.einsum('hqk,khd->qhd', prob_block, value_block, preferred_element_typ...  23.1 us
    all_to_all x1, blocking collectives, on_device(): lax.all_to_all(head_out, 'sp', split_axis=0, concat_axis=1, tiled=True)  19.6 us
    dot_general x8, matrix products, on_device(): jnp.einsum('td,kdc->ktc', part, columns, preferred_element_type=jnp.float32)  14.7 us
  transfers between devices with their start and end apart: 9, of which 5 were waited for; matrix products, arithmetic and copies ran while one was open for 46% of the time, Pallas kernels for 0%

profile of v1, /device:TPU:0, one launch (start us, length us, event | category | flops | bytes accessed | tf_op | source)
XLA Modules:
  0.0 491.1 jit_solution(16437094259261234924)
XLA Ops:
  9.5 32.0 %collective-permute-done = bf16[320,2048]{1,0:T(8,128)(2,1)S(1)} collective-permute-done((bf16[320,2048]{1,0:T(8,128)(2,1)}, bf16[320,2048]{1,0:T(8,128)(2,1)S(1)}, u32[]{:S(2)}, u32[]{:S(2)}) %collective-permute-start) | collective-permute-done | bytes 1310752 | tf_op jit(solution)/shard_map/ppermute | solution.py:72
  46.3 51.1 %collective-permute-done.1 = bf16[320,2048]{1,0:T(8,128)(2,1)} collective-permute-done((bf16[320,2048]{1,0:T(8,128)(2,1)S(1)}, bf16[320,2048]{1,0:T(8,128)(2,1)}, u32[]{:S(2)}, u32[]{:S(2)}) %collective-permute-start.1) | collective-permute-done | bytes 1310752 | tf_op jit(solution)/shard_map/ppermute | solution.py:72
  101.9 27.2 %collective-permute-start.5 = (bf16[320,2048]{1,0:T(8,128)(2,1)S(1)}, bf16[320,2048]{1,0:T(8,128)(2,1)}, u32[]{:S(2)}, u32[]{:S(2)}) collective-permute-start(bf16[320,2048]{1,0:T(8,128)(2,1)S(1)} %collective-permute-done.4), channel_id=1, source_target_pairs={{0,28},{4,0},{8,4},{12,8},{16,12},{20,16},{24,20},{28,24},{1,29},{... | collective-permute-start | bytes 3932168 | tf_op jit(solution)/shard_map/ppermute | solution.py:73
  129.1 26.2 %collective-permute-done.2 = bf16[320,2048]{1,0:T(8,128)(2,1)} collective-permute-done((bf16[320,2048]{1,0:T(8,128)(2,1)}, bf16[320,2048]{1,0:T(8,128)(2,1)}, u32[]{:S(2)}, u32[]{:S(2)}) %collective-permute-start.2) | collective-permute-done | bytes 1310752 | tf_op jit(solution)/shard_map/ppermute | solution.py:72
  157.8 7.9 %all_gather.10 = bf16[128,2048]{1,0:T(8,128)(2,1)} all-gather(bf16[128,512]{1,0:T(8,128)(2,1)} %param.17), channel_id=1, replica_groups=mesh['sp'=8,'dp'=4] {'dp'}, dimensions={1}, use_global_device_ids=true | all-gather | bytes 655360 | tf_op jit(solution)/shard_map/all_gather | solution.py:87
  165.7 27.7 %collective-permute-start.6 = (bf16[320,2048]{1,0:T(8,128)(2,1)}, bf16[320,2048]{1,0:T(8,128)(2,1)}, u32[]{:S(2)}, u32[]{:S(2)}) collective-permute-start(bf16[320,2048]{1,0:T(8,128)(2,1)} %collective-permute-done.5), channel_id=1, source_target_pairs={{0,28},{4,0},{8,4},{12,8},{16,12},{20,16},{24,20},{28,24},{1,29},{... | collective-permute-start | bytes 3932168 | tf_op jit(solution)/shard_map/ppermute | solution.py:73
  193.4 24.4 %collective-permute-done.3 = bf16[320,2048]{1,0:T(8,128)(2,1)} collective-permute-done((bf16[320,2048]{1,0:T(8,128)(2,1)}, bf16[320,2048]{1,0:T(8,128)(2,1)}, u32[]{:S(2)}, u32[]{:S(2)}) %collective-permute-start.3) | collective-permute-done | bytes 1310752 | tf_op jit(solution)/shard_map/ppermute | solution.py:72
  230.7 10.8 %collective-permute-done.6 = bf16[320,2048]{1,0:T(8,128)(2,1)} collective-permute-done((bf16[320,2048]{1,0:T(8,128)(2,1)}, bf16[320,2048]{1,0:T(8,128)(2,1)}, u32[]{:S(2)}, u32[]{:S(2)}) %collective-permute-start.6) | collective-permute-done | bytes 1310752 | tf_op jit(solution)/shard_map/ppermute | solution.py:73
  251.3 198.5 %while.33 = (s32[]{:T(128)}, f32[5,512,2,64]{1,3,2,0:T(8,128)}, s32[5]{0:T(128)S(1)}, bf16[2560,2,64]{0,2,1:T(8,128)(2,1)}, f32[2,2560]{1,0:T(2,128)}, /*index=5...) while((s32[]{:T(128)}, f32[5,512,2,64]{1,3,2,0:T(8,128)}, ...), condition=%wide.region_9.10_spmd, body=%wide.region_2.9_spmd.sunk | while | flops 143990816 | bytes 31886604 | solution.py:55
  254.8 5.3 %broadcast.99 = f32[2,512,2560]{1,2,0:T(8,128)} broadcast(f32[]{:T(128)} %constant.56.clone.6..sunk), dimensions={} | broadcast | bytes 10485764 | tf_op jit(solution)/shard_map/broadcast.5
  264.0 14.0 %divide_convert_fusion.2 = bf16[2,512,2560]{1,2,0:T(8,128)(2,1)} fusion(f32[2,512,2560]{1,2,0:T(8,128)} %get-tuple-element.368), kind=kOutput, calls=%fused_computation.16.clone.1 | output fusion | flops 7871486 | bytes 15728640 | tf_op jit(solution)/shard_map/while/body/eval_jaxpr/div | solution.py:42
  283.7 5.3 %broadcast.99 = f32[2,512,2560]{1,2,0:T(8,128)} broadcast(f32[]{:T(128)} %constant.56.clone.6..sunk), dimensions={} | broadcast | bytes 10485764 | tf_op jit(solution)/shard_map/broadcast.5
  289.1 7.6 %while.34 = (s32[]{:T(128)}, f32[2,512,2560]{1,2,0:T(8,128)}, s32[]{:T(128)}, bf16[2560,2,64]{0,2,1:T(8,128)(2,1)}, bf16[512,2,64]{0,2,1:T(8,128)(2,1)S(1)}, /*i...) while((s32[]{:T(128)}, f32[2,512,2560]{1,2,0:T(8,128)}, ...), condition=%wide.region_4.4_spmd.clone, body=%wide.region_3.3_spmd.clone.sunk | while | flops 68944904 | bytes 2909359 | solution.py:39
  296.7 14.0 %divide_convert_fusion.2 = bf16[2,512,2560]{1,2,0:T(8,128)(2,1)} fusion(f32[2,512,2560]{1,2,0:T(8,128)} %get-tuple-element.368), kind=kOutput, calls=%fused_computation.16.clone.1 | output fusion | flops 7871486 | bytes 15728640 | tf_op jit(solution)/shard_map/while/body/eval_jaxpr/div | solution.py:42
  323.3 11.5 %while.34 = (s32[]{:T(128)}, f32[2,512,2560]{1,2,0:T(8,128)}, s32[]{:T(128)}, bf16[2560,2,64]{0,2,1:T(8,128)(2,1)}, bf16[512,2,64]{0,2,1:T(8,128)(2,1)S(1)}, /*i...) while((s32[]{:T(128)}, f32[2,512,2560]{1,2,0:T(8,128)}, ...), condition=%wide.region_4.4_spmd.clone, body=%wide.region_3.3_spmd.clone.sunk | while | flops 68944904 | bytes 2909359 | solution.py:39
  334.8 14.0 %divide_convert_fusion.2 = bf16[2,512,2560]{1,2,0:T(8,128)(2,1)} fusion(f32[2,512,2560]{1,2,0:T(8,128)} %get-tuple-element.368), kind=kOutput, calls=%fused_computation.16.clone.1 | output fusion | flops 7871486 | bytes 15728640 | tf_op jit(solution)/shard_map/while/body/eval_jaxpr/div | solution.py:42
  363.0 15.4 %while.34 = (s32[]{:T(128)}, f32[2,512,2560]{1,2,0:T(8,128)}, s32[]{:T(128)}, bf16[2560,2,64]{0,2,1:T(8,128)(2,1)}, bf16[512,2,64]{0,2,1:T(8,128)(2,1)S(1)}, /*i...) while((s32[]{:T(128)}, f32[2,512,2560]{1,2,0:T(8,128)}, ...), condition=%wide.region_4.4_spmd.clone, body=%wide.region_3.3_spmd.clone.sunk | while | flops 68944904 | bytes 2909359 | solution.py:39
  378.4 14.0 %divide_convert_fusion.2 = bf16[2,512,2560]{1,2,0:T(8,128)(2,1)} fusion(f32[2,512,2560]{1,2,0:T(8,128)} %get-tuple-element.368), kind=kOutput, calls=%fused_computation.16.clone.1 | output fusion | flops 7871486 | bytes 15728640 | tf_op jit(solution)/shard_map/while/body/eval_jaxpr/div | solution.py:42
  392.4 6.3 %while.35 = (s32[]{:T(128)}, f32[512,2,64]{0,2,1:T(8,128)S(1)}, s32[]{:T(128)}, bf16[2560,2,64]{0,2,1:T(8,128)(2,1)S(1)}, bf16[2,512,2560]{1,2,0:T(8,128)(2,1)},...) while((s32[]{:T(128)}, f32[512,2,64]{0,2,1:T(8,128)S(1)}, s32[]{:T(128)}, ...), condition=%wide.region_8.8_spmd, body=%wide.region_7.7_spmd.sunk | while | flops 67174408 | bytes 1705099 | solution.py:53
  402.9 5.3 %broadcast.99 = f32[2,512,2560]{1,2,0:T(8,128)} broadcast(f32[]{:T(128)} %constant.56.clone.6..sunk), dimensions={} | broadcast | bytes 10485764 | tf_op jit(solution)/shard_map/broadcast.5
  408.2 19.1 %while.34 = (s32[]{:T(128)}, f32[2,512,2560]{1,2,0:T(8,128)}, s32[]{:T(128)}, bf16[2560,2,64]{0,2,1:T(8,128)(2,1)}, bf16[512,2,64]{0,2,1:T(8,128)(2,1)S(1)}, /*i...) while((s32[]{:T(128)}, f32[2,512,2560]{1,2,0:T(8,128)}, ...), condition=%wide.region_4.4_spmd.clone, body=%wide.region_3.3_spmd.clone.sunk | while | flops 68944904 | bytes 2909359 | solution.py:39
  427.3 14.0 %divide_convert_fusion.2 = bf16[2,512,2560]{1,2,0:T(8,128)(2,1)} fusion(f32[2,512,2560]{1,2,0:T(8,128)} %get-tuple-element.368), kind=kOutput, calls=%fused_computation.16.clone.1 | output fusion | flops 7871486 | bytes 15728640 | tf_op jit(solution)/shard_map/while/body/eval_jaxpr/div | solution.py:42
  441.3 7.9 %while.35 = (s32[]{:T(128)}, f32[512,2,64]{0,2,1:T(8,128)S(1)}, s32[]{:T(128)}, bf16[2560,2,64]{0,2,1:T(8,128)(2,1)S(1)}, bf16[2,512,2560]{1,2,0:T(8,128)(2,1)},...) while((s32[]{:T(128)}, f32[512,2,64]{0,2,1:T(8,128)S(1)}, s32[]{:T(128)}, ...), condition=%wide.region_8.8_spmd, body=%wide.region_7.7_spmd.sunk | while | flops 67174408 | bytes 1705099 | solution.py:53
  459.8 19.6 %all_to_all.16 = bf16[8,320,128]{2,1,0:T(8,128)(2,1)S(1)} all-to-all(bf16[8,320,128]{2,1,0:T(8,128)(2,1)S(1)} %copy.29), channel_id=1, replica_groups=mesh['sp'=8,'dp'=4] {'sp'}, dimensions={0} | all-to-all | bytes 1310720 | tf_op jit(solution)/shard_map/all_to_all | solution.py:102
  (168 shorter events, 171.0 us)
Async XLA Ops:
  6.5 159.2 %copy-start.2 = (f32[2,64]{1,0:T(2,128)S(1)}, f32[2,64]{1,0:T(2,128)}, u32[]{:S(2)}) copy-start(f32[2,64]{1,0:T(2,128)} %param.18) | copy-start | bytes 1540
  6.5 186.8 %all-gather.3.cloned.1.call-start = ((), (), s32[]{:S(2)}) async-start(), calls=%async_computation.1 | async-start | bytes 1966080 | tf_op jit(solution)/shard_map/all_gather | solution.py:86
  6.5 35.0 %collective-permute-start = (bf16[320,2048]{1,0:T(8,128)(2,1)}, bf16[320,2048]{1,0:T(8,128)(2,1)S(1)}, u32[]{:S(2)}, u32[]{:S(2)}) collective-permute-start(bf16[320,2048]{1,0:T(8,128)(2,1)} %bitcast.146), channel_id=1, source_target_pairs={{0,4},{4,8},{8,12},{12,16},{16,20},{20,24},{24,28},{28,0},{1,5},{5... | collective-permute-start | bytes 3932168 | tf_op jit(solution)/shard_map/ppermute | solution.py:72
  41.6 55.8 %collective-permute-start.1 = (bf16[320,2048]{1,0:T(8,128)(2,1)S(1)}, bf16[320,2048]{1,0:T(8,128)(2,1)}, u32[]{:S(2)}, u32[]{:S(2)}) collective-permute-start(bf16[320,2048]{1,0:T(8,128)(2,1)S(1)} %collective-permute-done), channel_id=1, source_target_pairs={{0,4},{4,8},{8,12},{12,16},{16,20},{20,24},{24,28},{28,0},{1,5},{5... | collective-permute-start | bytes 3932168 | tf_op jit(solution)/shard_map/ppermute | solution.py:72
  41.6 60.3 %collective-permute-start.4 = (bf16[320,2048]{1,0:T(8,128)(2,1)}, bf16[320,2048]{1,0:T(8,128)(2,1)S(1)}, u32[]{:S(2)}, u32[]{:S(2)}) collective-permute-start(bf16[320,2048]{1,0:T(8,128)(2,1)} %bitcast.147), channel_id=1, source_target_pairs={{0,28},{4,0},{8,4},{12,8},{16,12},{20,16},{24,20},{28,24},{1,29},{... | collective-permute-start | bytes 3932168 | tf_op jit(solution)/shard_map/ppermute | solution.py:73
  97.4 57.9 %collective-permute-start.2 = (bf16[320,2048]{1,0:T(8,128)(2,1)}, bf16[320,2048]{1,0:T(8,128)(2,1)}, u32[]{:S(2)}, u32[]{:S(2)}) collective-permute-start(bf16[320,2048]{1,0:T(8,128)(2,1)} %collective-permute-done.1), channel_id=1, source_target_pairs={{0,4},{4,8},{8,12},{12,16},{16,20},{20,24},{24,28},{28,0},{1,5},{5... | collective-permute-start | bytes 3932168 | tf_op jit(solution)/shard_map/ppermute | solution.py:72
  101.8 377.6 %all-gather.5.cloned.1.call-start = ((), (), s32[]{:S(2)}) async-start(), calls=%async_computation.2 | async-start | bytes 4718592 | tf_op jit(solution)/shard_map/all_gather | solution.py:105
  101.9 63.8 %collective-permute-start.5 = (bf16[320,2048]{1,0:T(8,128)(2,1)S(1)}, bf16[320,2048]{1,0:T(8,128)(2,1)}, u32[]{:S(2)}, u32[]{:S(2)}) collective-permute-start(bf16[320,2048]{1,0:T(8,128)(2,1)S(1)} %collective-permute-done.4), channel_id=1, source_target_pairs={{0,28},{4,0},{8,4},{12,8},{16,12},{20,16},{24,20},{28,24},{1,29},{... | collective-permute-start | bytes 3932168 | tf_op jit(solution)/shard_map/ppermute | solution.py:73
  155.3 62.5 %collective-permute-start.3 = (bf16[320,2048]{1,0:T(8,128)(2,1)}, bf16[320,2048]{1,0:T(8,128)(2,1)}, u32[]{:S(2)}, u32[]{:S(2)}) collective-permute-start(bf16[320,2048]{1,0:T(8,128)(2,1)} %collective-permute-done.2), channel_id=1, source_target_pairs={{0,4},{4,8},{8,12},{12,16},{16,20},{20,24},{24,28},{28,0},{1,5},{5... | collective-permute-start | bytes 3932168 | tf_op jit(solution)/shard_map/ppermute | solution.py:72
  165.7 75.8 %collective-permute-start.6 = (bf16[320,2048]{1,0:T(8,128)(2,1)}, bf16[320,2048]{1,0:T(8,128)(2,1)}, u32[]{:S(2)}, u32[]{:S(2)}) collective-permute-start(bf16[320,2048]{1,0:T(8,128)(2,1)} %collective-permute-done.5), channel_id=1, source_target_pairs={{0,28},{4,0},{8,4},{12,8},{16,12},{20,16},{24,20},{28,24},{1,29},{... | collective-permute-start | bytes 3932168 | tf_op jit(solution)/shard_map/ppermute | solution.py:73
  193.4 27.5 %copy-start.3 = (bf16[3,2048,128]{2,1,0:T(8,128)(2,1)S(1)}, bf16[3,2048,128]{2,1,0:T(8,128)(2,1)}, u32[]{:S(2)}) copy-start(bf16[3,2048,128]{2,1,0:T(8,128)(2,1)} %all-gather.3.cloned.1.call-done) | copy-start | bytes 4718596
  225.3 1.3 copy-start.4
  452.0 2.0 copy-start.1
  455.4 1.8 copy-start
Sparse Core Ops, SparseCore 0:
  102.0 18.2 all-gather.2
  165.8 97.7 all-gather.4
